TPU v7x, 32 devices: a whole 2x2x4 slice. The times are simulated.
32 devices in a mesh: sp: 16 (over z, y, x), dp: 2 (over core).
Axes of the slice: x: 2, y: 2, z: 4, core: 2. Of those that a mesh axis runs over, the one named last changes fastest.
Arguments:
- gate_input: bfloat16 [2, 3072, 1024], P('dp', 'sp'), may hold values from -6 to 6
- value_input: bfloat16 [2, 3072, 1024], P('dp', 'sp'), may hold values from -6 to 6
- norm_gain: float32 [1024], replicated, may hold values from 0.1 to 1.9
- norm_bias: float32 [1024], replicated, may hold values from -3 to 3
- mix_weight: bfloat16 [16, 1024, 1024], P('sp', 'dp'), may hold values from -0.1875 to 0.1875
- mix_bias: float32 [16, 1024], P('sp'), may hold values from 0.1 to 1.9
Outputs:
- gated: bfloat16 [2, 3072, 1024], P('dp', 'sp')
All inputs are finite; a program needn't handle non-finite values.
Results may differ from a plain program's by a relative error of at most 0.0053.
Values may be sent and summed in bfloat16 or wider, within the bound.
A program may use at most 64 MiB of HBM per device.

v0:
```python
import jax
import jax.numpy as jnp
from jax import lax
from jax.sharding import PartitionSpec as P

GROUP_DIM = 64
SPAN = 1024


epsilon = 1e-05


def local(gate_input, value_input, norm_gain, norm_bias, mix_weight, mix_bias):
    token_rows = value_input.shape[1]
    channels = value_input.shape[2]
    act_value = jax.nn.gelu(value_input[0].astype(jnp.float32))
    centre = jnp.mean(act_value, axis=-1, keepdims=True)
    shifted = act_value - centre
    variance = jnp.mean(shifted * shifted, axis=-1, keepdims=True)
    normed = (shifted * lax.rsqrt(variance + epsilon) * norm_gain + norm_bias).astype(jnp.bfloat16)
    normed_group = lax.all_to_all(normed, "sp", split_axis=1, concat_axis=0, tiled=True)
    positions = normed_group.shape[0]
    group_count = mix_weight.shape[0]
    blocks = normed_group.reshape(positions // SPAN, SPAN, group_count, GROUP_DIM)
    columns = lax.broadcasted_iota(jnp.int32, (1, SPAN), 1)
    weight_rows = lax.all_gather(mix_weight, "dp", axis=1, tiled=True)
    row_count = weight_rows.shape[1]
    rows_index = lax.broadcasted_iota(jnp.int32, (row_count, 1), 0)
    masked = jnp.where((columns <= rows_index)[None], weight_rows, jnp.zeros_like(weight_rows))
    summed = jnp.einsum("gqp,npgc->nqgc", masked, blocks, preferred_element_type=jnp.float32)
    mixed_blocks = (summed + mix_bias.T[None, :, :, None]).astype(jnp.bfloat16)
    mixed_flat = lax.optimization_barrier(mixed_blocks.reshape(positions, group_count * GROUP_DIM))
    returned = lax.all_to_all(mixed_flat, "sp", split_axis=0, concat_axis=1, tiled=True)
    gated_rows = (
        jax.nn.gelu(gate_input[0].astype(jnp.float32)) * returned.astype(jnp.float32)
    ).astype(jnp.bfloat16)
    return gated_rows.reshape(1, token_rows, channels)


def solution(mesh):
    in_specs = (
        P("dp", "sp", None),
        P("dp", "sp", None),
        P(),
        P(),
        P("sp", "dp", None),
        P("sp", None),
    )
    out_specs = P("dp", "sp", None)
    return jax.shard_map(local, mesh=mesh, in_specs=in_specs, out_specs=out_specs, check_vma=False)
```

profile of v0, /device:TPU:0, one launch (start us, length us, event | category | flops | bytes accessed | tf_op | source)
XLA Modules:
  0.0 65.9 jit_solution(4898811515599246371)
XLA Ops:
  6.5 0.0 all-gather.2.cloned.1.call-start
  6.5 0.7 %all-gather.2.cloned.1.call-update = ((bf16[1,512,1024]{2,1,0:T(8,128)(2,1)}), bf16[1,1024,1024]{2,1,0:T(8,128)(2,1)}) async-update(((), (), s32[]{:S(2)}) %all-gather.2.cloned.1.call-start, bf16[1,512,1024]{2,1,0:T(8,128)(2,1)} %param.10) | async-update | bytes 4194328
  7.3 1.2 %copy.21 = bf16[1,192,1024]{1,2,0:T(8,128)(2,1)S(1)} copy(bf16[1,192,1024]{2,1,0:T(8,128)(2,1)} %param.7) | data formatting | bytes 786432 | tf_op args[1]
  8.5 0.8 %add.61 = f32[16,64]{1,0:T(8,128)S(1)} reshape(f32[1024]{0:T(1024)} %param.9) | data formatting | bytes 8192 | tf_op jit(solution)/shard_map/add | solution.py:20
  9.2 0.8 %mul.82 = f32[16,64]{1,0:T(8,128)S(1)} reshape(f32[1024]{0:T(1024)} %param.8) | data formatting | bytes 8192 | tf_op jit(solution)/shard_map/mul | solution.py:20
  10.0 0.4 fusion.43
  10.4 0.5 multiply_reduce_fusion
  10.9 0.0 copy-start.1
  10.9 0.5 fusion.35
  11.4 23.2 %all_to_all.26 = bf16[192,16,64]{0,2,1:T(8,128)(2,1)S(1)} all-to-all(bf16[192,16,64]{0,2,1:T(8,128)(2,1)S(1)} %fusion.35), channel_id=1, replica_groups=mesh['sp'=16,'dp'=2] {'sp'}, dimensions={1} | all-to-all | bytes 786432 | tf_op jit(solution)/shard_map/all_to_all | solution.py:21
  34.6 0.3 copy.22
  34.9 0.7 %reshape.90 = bf16[3,1024,64]{1,0,2:T(4,128)(2,1)S(1)} reshape(bf16[16,192,64]{1,0,2:T(8,128)(2,1)S(1)} %copy.22) | data formatting | bytes 786432 | tf_op jit(solution)/shard_map/reshape.1
  35.6 0.0 all-gather.2.cloned.1.call-done
  35.7 0.0 copy-done.1
  35.7 2.3 %fusion.13 = bf16[3,1024,1,64]{1,3,0,2:T(8,128)(2,1)S(1)} fusion(bf16[1,1024,1024]{2,1,0:T(8,128)(2,1)} %all-gather.2.cloned.1.call-done, bf16[3,1024,64]{1,0,2:T(4,128)(2,1)S(1)} %reshape.90, f32[1024]{0:T(1024)S(1)} %bitcast.49), kind=kOutput, calls=%fused_computation.13 | convolution fusion | flops 405143552 | bytes 2887680 | tf_op jit(solution)/shard_map/gqp,npgc->nqgc/dot_general | solution.py:30
  38.0 0.3 copy.24
  38.3 0.2 copy.27
  38.5 0.6 all_to_all.22
  39.1 0.2 copy.25
  39.3 0.0 copy-start
  39.3 18.3 %all_to_all.27 = bf16[16,192,64]{1,2,0:T(8,128)(2,1)S(1)} all-to-all(bf16[16,192,64]{1,2,0:T(8,128)(2,1)S(1)} %copy.25), channel_id=1, replica_groups=mesh['sp'=16,'dp'=2] {'sp'}, dimensions={0} | all-to-all | bytes 786432 | tf_op jit(solution)/shard_map/all_to_all | solution.py:33
  57.6 0.1 convert_element_type.61
  57.7 0.3 copy.26
  58.0 0.0 copy-done
  58.0 1.0 %fusion.42 = bf16[1,192,1024]{2,1,0:T(8,128)(2,1)} fusion(f32[1,192,1024]{2,1,0:T(8,128)S(1)} %copy.26, bf16[1,192,1024]{2,1,0:T(8,128)(2,1)S(1)} %copy-done), kind=kLoop, calls=%fused_computation.41 | loop fusion | flops 2162688 | bytes 1572864 | tf_op jit(solution)/shard_map/convert_element_type | solution.py:36
  (2 shorter events, 0.0 us)
Async XLA Ops:
  6.5 29.1 %all-gather.2.cloned.1.call-start = ((), (), s32[]{:S(2)}) async-start(), calls=%async_computation.2 | async-start | bytes 3145728 | tf_op jit(solution)/shard_map/all_gather | solution.py:26
  10.9 24.8 %copy-start.1 = (f32[1,1024]{1,0:T(1,128)S(1)}, f32[1,1024]{1,0:T(1,128)}, u32[]{:S(2)}) copy-start(f32[1,1024]{1,0:T(1,128)} %param.11) | copy-start | bytes 12292
  39.3 18.8 %copy-start = (bf16[1,192,1024]{2,1,0:T(8,128)(2,1)S(1)}, bf16[1,192,1024]{2,1,0:T(8,128)(2,1)}, u32[]{:S(2)}) copy-start(bf16[1,192,1024]{2,1,0:T(8,128)(2,1)} %param.6) | copy-start | bytes 1179652
Sparse Core Ops, SparseCore 0:
  8.9 13.2 all-gather.1
where the time goes:
time: 66.2 us; the launch traced here: 65.9 us
  blocking collectives  41.5 us (63%)
  between operations  13.5 us (20%)
  local copies, waits for them, and re-layouts  5.31 us (8%)
  other arithmetic  2.55 us (4%)
  matrix products  2.29 us (3%)
  waiting for transfers between devices  0.73 us (1%)
    all_to_all x1, blocking collectives, local(): lax.all_to_all(normed, 'sp', split_axis=1, concat_axis=0, tiled=True)  23.2 us
    all_to_all x1, blocking collectives, local(): lax.all_to_all(mixed_flat, 'sp', split_axis=0, concat_axis=1, tiled=True)  18.3 us
    dot_general x1, matrix products, local(): jnp.einsum('gqp,npgc->nqgc', masked, blocks, preferred_element_type=jnp.f...  2.29 us
    unnamed x6, local copies, waits for them, and re-layouts  1.37 us
  transfers between devices with their start and end apart: 1, of which 0 were waited for; matrix products, arithmetic and copies ran while one was open for 8% of the time, Pallas kernels for 0%

commit v1 on v0

v1 whole, which is shorter than its diff:
```python
import functools
import math

import jax
import jax.numpy as jnp
from jax import lax
from jax.experimental import pallas as pl
from jax.experimental.pallas import tpu as pltpu
from jax.sharding import PartitionSpec as P

GROUP_DIM = 64
SPAN = 1024
LANES = 128
ROWS = 16

epsilon = 1e-05


def partner(me, k, n):
    if n & (n - 1):
        return lax.rem(me + k, n)
    out = 0
    bit = 1
    while bit < n:
        flip = 1 if k & bit else 0
        out = out + ((me // bit + flip) % 2) * bit
        bit *= 2
    return out


def segments(source, rows):
    half = rows // 2
    runs = []
    for a in range(2):
        r = 0
        while r < half:
            position = source * rows + a * half + r
            block, p = divmod(position, SPAN)
            length = min(half - r, SPAN - p)
            runs.append((a, r, length, block, p))
            r += length
    return runs


def kernel(
    n, dp, tile, value, gate, gain, nbias, weight, mbias, out,
    vbuf, gbuf, gainbuf, nbiasbuf, mbiasbuf, act, full, bcol, s1, r1, xbuf, ybuf, s2, r2, obuf,
    load_sem, wsend, wrecv, send1, recv1, send2, recv2, out_sem,
):
    me = lax.axis_index("sp")
    row = lax.axis_index("dp")
    tokens, channels = vbuf.shape
    half = tokens // 2
    wrows = weight.shape[0]
    pairs = channels // LANES

    load_value = pltpu.make_async_copy(value, vbuf, load_sem.at[0])
    load_gain = pltpu.make_async_copy(gain, gainbuf, load_sem.at[1])
    load_nbias = pltpu.make_async_copy(nbias, nbiasbuf, load_sem.at[2])
    load_gate = pltpu.make_async_copy(gate, gbuf, load_sem.at[3])
    load_mbias = pltpu.make_async_copy(mbias, mbiasbuf, load_sem.at[4])
    own_rows = full.at[pl.ds(pl.multiple_of(row * wrows, wrows), wrows), :]
    load_weight = pltpu.make_async_copy(weight, own_rows, load_sem.at[5])
    load_value.start()
    load_gain.start()
    load_nbias.start()
    load_weight.start()
    load_mbias.start()
    load_gate.start()

    barrier = pltpu.get_barrier_semaphore()
    order = list(range(n - 1, 0, -1))
    peers = {k: partner(me, k, n) for k in order}
    for k in order:
        pl.semaphore_signal(barrier, inc=1, device_id={"sp": peers[k]})
    for j in range(1, dp):
        pl.semaphore_signal(barrier, inc=1, device_id={"dp": lax.rem(row + j, dp)})

    load_value.wait()
    load_gain.wait()
    load_nbias.wait()
    lower = lax.broadcasted_iota(jnp.int32, (ROWS, LANES), 1) < GROUP_DIM

    def normed_rows(start):
        x = jax.nn.gelu(vbuf[pl.ds(start, ROWS), :].astype(jnp.float32))
        shifted = x - jnp.mean(x, axis=-1, keepdims=True)
        variance = jnp.mean(shifted * shifted, axis=-1, keepdims=True)
        return shifted * lax.rsqrt(variance + epsilon) * gainbuf[...] + nbiasbuf[...]

    for r in range(0, half, ROWS):
        top = normed_rows(r)
        bottom = normed_rows(half + r)
        for j in range(pairs):
            t = top[:, j * LANES:(j + 1) * LANES]
            b = bottom[:, j * LANES:(j + 1) * LANES]
            s1[2 * j, pl.ds(r, ROWS), :] = jnp.where(lower, t, pltpu.roll(b, GROUP_DIM, 1)).astype(jnp.bfloat16)
            s1[2 * j + 1, pl.ds(r, ROWS), :] = jnp.where(lower, pltpu.roll(t, GROUP_DIM, 1), b).astype(jnp.bfloat16)

    pl.semaphore_wait(barrier, n - 1 + dp - 1)

    def exchange(src, dst, send_sem, recv_sem):
        copies = []
        for k in order:
            copy = pltpu.make_async_remote_copy(
                src_ref=src.at[peers[k]], dst_ref=dst.at[me], send_sem=send_sem.at[k],
                recv_sem=recv_sem.at[me], device_id={"sp": peers[k]},
            )
            copy.start()
            copies.append(copy)
        pltpu.make_async_copy(src.at[me], dst.at[me], recv_sem.at[me]).start()
        return copies

    sends = exchange(s1, r1, send1, recv1)
    wcopies = []
    for j in range(1, dp):
        copy = pltpu.make_async_remote_copy(
            src_ref=weight, dst_ref=own_rows, send_sem=wsend.at[j], recv_sem=wrecv.at[row],
            device_id={"dp": lax.rem(row + j, dp)},
        )
        copy.start()
        wcopies.append(copy)

    load_gate.wait()
    for r in range(0, tokens, ROWS):
        act[pl.ds(r, ROWS), :] = jax.nn.gelu(gbuf[pl.ds(r, ROWS), :].astype(jnp.float32))
    load_mbias.wait()
    for q in range(0, SPAN, LANES):
        bcol[pl.ds(q, LANES), :] = jnp.transpose(jnp.broadcast_to(mbiasbuf[:, q:q + LANES], (LANES, LANES)))
    xbuf[:, xbuf.shape[1] - LANES:] = jnp.zeros((SPAN, LANES), jnp.bfloat16)

    load_weight.wait()
    for j in range(1, dp):
        other = lax.rem(row + j, dp)
        rows_of = full.at[pl.ds(pl.multiple_of(other * wrows, wrows), wrows), :]
        pltpu.make_async_copy(weight, rows_of, wrecv.at[other]).wait()
    for q in range(0, SPAN, tile):
        block = full[pl.ds(q, tile), pl.ds(q, tile)].astype(jnp.float32)
        keep = lax.broadcasted_iota(jnp.int32, (tile, tile), 1) <= lax.broadcasted_iota(jnp.int32, (tile, tile), 0)
        full[pl.ds(q, tile), pl.ds(q, tile)] = jnp.where(keep, block, 0.0).astype(jnp.bfloat16)

    for s in range(n):
        pltpu.make_async_copy(s1.at[s], r1.at[s], recv1.at[s]).wait()
        for a, r, length, block, p in segments(s, tokens):
            xbuf[p:p + length, block * GROUP_DIM:(block + 1) * GROUP_DIM] = (
                r1[s, r:r + length, a * GROUP_DIM:(a + 1) * GROUP_DIM]
            )

    for q in range(0, SPAN, tile):
        summed = jnp.dot(full[q:q + tile, :q + tile], xbuf[:q + tile, :], preferred_element_type=jnp.float32)
        column = bcol[q:q + tile, :]
        for j in range(0, xbuf.shape[1], LANES):
            ybuf[q:q + tile, j:j + LANES] = (summed[:, j:j + LANES] + column).astype(jnp.bfloat16)

    for s in range(n):
        for a, r, length, block, p in segments(s, tokens):
            s2[s, r:r + length, a * GROUP_DIM:(a + 1) * GROUP_DIM] = (
                ybuf[p:p + length, block * GROUP_DIM:(block + 1) * GROUP_DIM]
            )
    returns = exchange(s2, r2, send2, recv2)

    stores = []
    for j in range(pairs):
        for s in (2 * j, 2 * j + 1):
            pltpu.make_async_copy(s2.at[s], r2.at[s], recv2.at[s]).wait()
        cols = slice(j * LANES, (j + 1) * LANES)
        for r in range(0, half, ROWS):
            e = r2[2 * j, r:r + ROWS, :].astype(jnp.float32)
            o = r2[2 * j + 1, r:r + ROWS, :].astype(jnp.float32)
            top = jnp.where(lower, e, pltpu.roll(o, GROUP_DIM, 1))
            bottom = jnp.where(lower, pltpu.roll(e, GROUP_DIM, 1), o)
            obuf[r:r + ROWS, cols] = (act[r:r + ROWS, cols] * top).astype(jnp.bfloat16)
            obuf[half + r:half + r + ROWS, cols] = (act[half + r:half + r + ROWS, cols] * bottom).astype(jnp.bfloat16)
    store = pltpu.make_async_copy(obuf, out, out_sem.at[0])
    store.start()
    for copy in sends + wcopies + returns:
        copy.wait_send()
    store.wait()


def solution(mesh):
    n, dp = mesh.shape["sp"], mesh.shape["dp"]

    def local(gate_input, value_input, norm_gain, norm_bias, mix_weight, mix_bias):
        _, tokens, channels = value_input.shape
        groups, wrows, span = mix_weight.shape
        assert groups == 1 and span == SPAN and channels == n * GROUP_DIM and tokens % (2 * ROWS) == 0
        half = tokens // 2
        blocks = n * tokens // SPAN
        width = -(-blocks * GROUP_DIM // LANES) * LANES
        packed = (n, half, 2 * GROUP_DIM)
        anywhere = pl.BlockSpec(memory_space=pl.ANY)
        bf16, f32 = jnp.bfloat16, jnp.float32
        dma = pltpu.SemaphoreType.DMA
        result = pl.pallas_call(
            functools.partial(kernel, n, dp, 256),
            out_shape=jax.ShapeDtypeStruct((tokens, channels), bf16),
            in_specs=[anywhere] * 6,
            out_specs=anywhere,
            scratch_shapes=[
                pltpu.VMEM((tokens, channels), bf16),
                pltpu.VMEM((tokens, channels), bf16),
                pltpu.VMEM((1, channels), f32),
                pltpu.VMEM((1, channels), f32),
                pltpu.VMEM((1, SPAN), f32),
                pltpu.VMEM((tokens, channels), f32),
                pltpu.VMEM((SPAN, SPAN), bf16),
                pltpu.VMEM((SPAN, LANES), f32),
                pltpu.VMEM(packed, bf16),
                pltpu.VMEM(packed, bf16),
                pltpu.VMEM((SPAN, width), bf16),
                pltpu.VMEM((SPAN, width), bf16),
                pltpu.VMEM(packed, bf16),
                pltpu.VMEM(packed, bf16),
                pltpu.VMEM((tokens, channels), bf16),
                dma((6,)),
                dma((dp,)),
                dma((dp,)),
                dma((n,)),
                dma((n,)),
                dma((n,)),
                dma((n,)),
                dma((1,)),
            ],
            compiler_params=pltpu.CompilerParams(collective_id=0, has_side_effects=True),
        )(
            value_input[0], gate_input[0], norm_gain.reshape(1, channels), norm_bias.reshape(1, channels),
            mix_weight[0], mix_bias,
        )
        return result.reshape(1, tokens, channels)

    in_specs = (
        P("dp", "sp", None),
        P("dp", "sp", None),
        P(),
        P(),
        P("sp", "dp", None),
        P("sp", None),
    )
    return jax.shard_map(local, mesh=mesh, in_specs=in_specs, out_specs=P("dp", "sp", None), check_vma=False)
```

time: 66.2 us -> 30 us (0.45)
  blocking collectives: 41.5 us -> 0 us
  Pallas kernels: 0 us -> 28 us
  between operations: 13.5 us -> 0.01 us
  local copies, waits for them, and re-layouts: 5.31 us -> 1.77 us
  other arithmetic: 2.55 us -> 0 us
  matrix products: 2.29 us -> 0 us
  waiting for transfers between devices: 0.73 us -> 0 us
    all_to_all x2 -> x0, blocking collectives: 41.5 us -> none  [the longest x1 23.2 us: local(): lax.all_to_all(normed, 'sp', split_axis=1, concat_axis=0, tiled=True)]
    pallas_call x0 -> x1, Pallas kernels: none -> 28 us  [local(): pl.pallas_call(functools.partial(kernel, n, dp, 256), out_shape=jax.Shape...]
    dot_general x1 -> x0, matrix products: 2.29 us -> none  [local(): jnp.einsum('gqp,npgc->nqgc', masked, blocks, preferred_element_type=jnp.f...]
    convert_element_type x3 -> x0, other arithmetic: 1.65 us -> none  [the longest x1 1.05 us: local(): gated_rows = (jax.nn.gelu(gate_input[0].astype(jnp.float32)) * returned.a...]
    all_to_all x3 -> x0, local copies, waits for them, and re-layouts: 1.05 us -> none  [the longest x2 0.76 us: local(): lax.all_to_all(mixed_flat, 'sp', split_axis=0, concat_axis=1, tiled=True)]
    reduce_sum x2 -> x0, other arithmetic: 0.89 us -> none  [the longest x1 0.48 us: local(): variance = jnp.mean(shifted * shifted, axis=-1, keepdims=True)]
    add x1 -> x0, local copies, waits for them, and re-layouts: 0.76 us -> none  [local(): shifted * lax.rsqrt(variance + epsilon) * norm_gain + norm_bias]
    mul x1 -> x0, local copies, waits for them, and re-layouts: 0.75 us -> none  [local(): shifted * lax.rsqrt(variance + epsilon) * norm_gain + norm_bias]
  transfers between devices with their start and end apart: 1 -> 0, of which waited for: 0 -> 0; matrix products, arithmetic and copies ran while one was open for 8% -> 0% of each run, Pallas kernels for 0% -> 0%
where the time goes in v1:
time: 30 us; the launch traced here: 29.8 us
  Pallas kernels  28 us (93%)
  local copies, waits for them, and re-layouts  1.77 us (6%)
    pallas_call x1, Pallas kernels, local(): pl.pallas_call(functools.partial(kernel, n, dp, 256), out_shape=jax.Shape...  28 us
    unnamed x1, local copies, waits for them, and re-layouts  1.77 us

profile of v1, /device:TPU:0, one launch (start us, length us, event | category | flops | bytes accessed | tf_op | source)
XLA Modules:
  0.0 29.8 jit_solution(4771784761650454475)
XLA Ops:
  0.0 28.0 %shard_map.64 = bf16[192,1024]{1,0:T(8,128)(2,1)} custom-call(bf16[192,1024]{1,0:T(8,128)(2,1)} %bitcast.8, bf16[192,1024]{1,0:T(8,128)(2,1)} %bitcast.9, f32[1,1024]{1,0:T(1,128)} %bitcast.10, f32[1,1024]{1,0:T(1,128)} %bitcast.11, bf16[512,1024]{1,0:T(8,128)(2,1)} %bitcast.7, f32[1,1024]{1,0:T(1,128)} %mbias.1), custom_call_target="tpu_custom_call" | custom-call | tf_op jit(solution)/shard_map/pallas_call | solution.py:194
  28.0 1.8 %copy.8 = bf16[1,192,1024]{2,1,0:T(8,128)(2,1)} copy(bf16[1,192,1024]{2,1,0:T(8,128)(2,1)} %bitcast.6) | data formatting | bytes 786432

commit v2 on v1

--- a/solution.py
+++ b/solution.py
@@ -44,8 +44,8 @@
 
 def kernel(
     n, dp, tile, value, gate, gain, nbias, weight, mbias, out,
-    vbuf, gbuf, gainbuf, nbiasbuf, mbiasbuf, act, full, bcol, s1, r1, xbuf, ybuf, s2, r2, obuf,
-    load_sem, wsend, wrecv, send1, recv1, send2, recv2, out_sem,
+    vbuf, gbuf, gainbuf, nbiasbuf, mbiasbuf, act, full, bcol, s1, r1, xbuf, ybuf, s2, r2,
+    load_sem, wsend, wrecv, send1, recv1, send2, recv2,
 ):
     me = lax.axis_index("sp")
     row = lax.axis_index("dp")
@@ -158,7 +158,6 @@
             )
     returns = exchange(s2, r2, send2, recv2)
 
-    stores = []
     for j in range(pairs):
         for s in (2 * j, 2 * j + 1):
             pltpu.make_async_copy(s2.at[s], r2.at[s], recv2.at[s]).wait()
@@ -168,13 +167,10 @@
             o = r2[2 * j + 1, r:r + ROWS, :].astype(jnp.float32)
             top = jnp.where(lower, e, pltpu.roll(o, GROUP_DIM, 1))
             bottom = jnp.where(lower, pltpu.roll(e, GROUP_DIM, 1), o)
-            obuf[r:r + ROWS, cols] = (act[r:r + ROWS, cols] * top).astype(jnp.bfloat16)
-            obuf[half + r:half + r + ROWS, cols] = (act[half + r:half + r + ROWS, cols] * bottom).astype(jnp.bfloat16)
-    store = pltpu.make_async_copy(obuf, out, out_sem.at[0])
-    store.start()
+            out[r:r + ROWS, cols] = (act[r:r + ROWS, cols] * top).astype(jnp.bfloat16)
+            out[half + r:half + r + ROWS, cols] = (act[half + r:half + r + ROWS, cols] * bottom).astype(jnp.bfloat16)
     for copy in sends + wcopies + returns:
         copy.wait_send()
-    store.wait()
 
 
 def solution(mesh):
@@ -193,9 +189,9 @@
         dma = pltpu.SemaphoreType.DMA
         result = pl.pallas_call(
             functools.partial(kernel, n, dp, 256),
-            out_shape=jax.ShapeDtypeStruct((tokens, channels), bf16),
+            out_shape=pltpu.VMEM((tokens, channels), bf16),
             in_specs=[anywhere] * 6,
-            out_specs=anywhere,
+            out_specs=pl.BlockSpec(memory_space=pltpu.VMEM),
             scratch_shapes=[
                 pltpu.VMEM((tokens, channels), bf16),
                 pltpu.VMEM((tokens, channels), bf16),
@@ -211,7 +207,6 @@
                 pltpu.VMEM((SPAN, width), bf16),
                 pltpu.VMEM(packed, bf16),
                 pltpu.VMEM(packed, bf16),
-                pltpu.VMEM((tokens, channels), bf16),
                 dma((6,)),
                 dma((dp,)),
                 dma((dp,)),
@@ -219,7 +214,6 @@
                 dma((n,)),
                 dma((n,)),
                 dma((n,)),
-                dma((1,)),
             ],
             compiler_params=pltpu.CompilerParams(collective_id=0, has_side_effects=True),
         )(

time: 30 us -> 28.2 us (0.940)
  local copies, waits for them, and re-layouts: 1.77 us -> 0.75 us
  Pallas kernels: 28 us -> 27.3 us
    unnamed x1, local copies, waits for them, and re-layouts: 1.77 us -> 0.75 us
    pallas_call x1, Pallas kernels: 28 us -> 27.3 us  [local(): pl.pallas_call(functools.partial(kernel, n, dp, 256), out_shape=pltpu.VME...]
where the time goes in v2:
time: 28.2 us; the launch traced here: 28.1 us
  Pallas kernels  27.3 us (97%)
  local copies, waits for them, and re-layouts  0.75 us (3%)
    pallas_call x1, Pallas kernels, local(): pl.pallas_call(functools.partial(kernel, n, dp, 256), out_shape=pltpu.VME...  27.3 us
    unnamed x1, local copies, waits for them, and re-layouts  0.75 us

profile of v2, /device:TPU:0, one launch (start us, length us, event | category | flops | bytes accessed | tf_op | source)
XLA Modules:
  0.0 28.1 jit_solution(15695361112221953370)
XLA Ops:
  0.0 27.3 %shard_map.64 = bf16[192,1024]{1,0:T(8,128)(2,1)S(1)} custom-call(bf16[192,1024]{1,0:T(8,128)(2,1)} %bitcast.8, bf16[192,1024]{1,0:T(8,128)(2,1)} %bitcast.9, f32[1,1024]{1,0:T(1,128)} %bitcast.10, f32[1,1024]{1,0:T(1,128)} %bitcast.11, bf16[512,1024]{1,0:T(8,128)(2,1)} %bitcast.7, f32[1,1024]{1,0:T(1,128)} %mbias.1), custom_call_target="tpu_custom_call" | custom-call | tf_op jit(solution)/shard_map/pallas_call | solution.py:190
  27.3 0.7 %copy.8 = bf16[1,192,1024]{2,1,0:T(8,128)(2,1)} copy(bf16[1,192,1024]{2,1,0:T(8,128)(2,1)S(1)} %bitcast.6) | data formatting | bytes 786432

commit v3 on v2

--- a/solution.py
+++ b/solution.py
@@ -22,8 +22,7 @@
     out = 0
     bit = 1
     while bit < n:
-        flip = 1 if k & bit else 0
-        out = out + ((me // bit + flip) % 2) * bit
+        out = out + ((me // bit + k // bit) % 2) * bit
         bit *= 2
     return out
 
@@ -69,10 +68,10 @@
     load_gate.start()
 
     barrier = pltpu.get_barrier_semaphore()
-    order = list(range(n - 1, 0, -1))
-    peers = {k: partner(me, k, n) for k in order}
-    for k in order:
-        pl.semaphore_signal(barrier, inc=1, device_id={"sp": peers[k]})
+    late = 2 * ((me * tokens + half) % SPAN) // SPAN
+    peers = [partner(me, k + late * (n - 2 * k), n) for k in range(n - 1, 0, -1)]
+    for peer in peers:
+        pl.semaphore_signal(barrier, inc=1, device_id={"sp": peer})
     for j in range(1, dp):
         pl.semaphore_signal(barrier, inc=1, device_id={"dp": lax.rem(row + j, dp)})
 
@@ -98,19 +97,20 @@
 
     pl.semaphore_wait(barrier, n - 1 + dp - 1)
 
-    def exchange(src, dst, send_sem, recv_sem):
-        copies = []
-        for k in order:
-            copy = pltpu.make_async_remote_copy(
-                src_ref=src.at[peers[k]], dst_ref=dst.at[me], send_sem=send_sem.at[k],
-                recv_sem=recv_sem.at[me], device_id={"sp": peers[k]},
-            )
-            copy.start()
-            copies.append(copy)
-        pltpu.make_async_copy(src.at[me], dst.at[me], recv_sem.at[me]).start()
-        return copies
-
-    sends = exchange(s1, r1, send1, recv1)
+    sends = []
+    for k, peer in enumerate(peers):
+        copy = pltpu.make_async_remote_copy(
+            src_ref=s1.at[peer], dst_ref=r1.at[me], send_sem=send1.at[k], recv_sem=recv1.at[me], device_id={"sp": peer},
+        )
+        copy.start()
+        sends.append(copy)
+    pltpu.make_async_copy(s1.at[me], r1.at[me], recv1.at[me]).start()
+
+    def give_back(s):
+        return pltpu.make_async_remote_copy(
+            src_ref=s2.at[s], dst_ref=r2.at[me], send_sem=send2.at[s], recv_sem=recv2.at[me], device_id={"sp": s},
+        )
+
     wcopies = []
     for j in range(1, dp):
         copy = pltpu.make_async_remote_copy(
@@ -138,25 +138,41 @@
         keep = lax.broadcasted_iota(jnp.int32, (tile, tile), 1) <= lax.broadcasted_iota(jnp.int32, (tile, tile), 0)
         full[pl.ds(q, tile), pl.ds(q, tile)] = jnp.where(keep, block, 0.0).astype(jnp.bfloat16)
 
-    for s in range(n):
-        pltpu.make_async_copy(s1.at[s], r1.at[s], recv1.at[s]).wait()
-        for a, r, length, block, p in segments(s, tokens):
-            xbuf[p:p + length, block * GROUP_DIM:(block + 1) * GROUP_DIM] = (
-                r1[s, r:r + length, a * GROUP_DIM:(a + 1) * GROUP_DIM]
-            )
-
+    waited, returned = set(), set()
     for q in range(0, SPAN, tile):
+        for s in range(n):
+            runs = segments(s, tokens)
+            if s in waited or min(p for _, _, _, _, p in runs) >= q + tile:
+                continue
+            waited.add(s)
+            pltpu.make_async_copy(s1.at[s], r1.at[s], recv1.at[s]).wait()
+            for a, r, length, block, p in runs:
+                xbuf[p:p + length, block * GROUP_DIM:(block + 1) * GROUP_DIM] = (
+                    r1[s, r:r + length, a * GROUP_DIM:(a + 1) * GROUP_DIM]
+                )
         summed = jnp.dot(full[q:q + tile, :q + tile], xbuf[:q + tile, :], preferred_element_type=jnp.float32)
         column = bcol[q:q + tile, :]
         for j in range(0, xbuf.shape[1], LANES):
             ybuf[q:q + tile, j:j + LANES] = (summed[:, j:j + LANES] + column).astype(jnp.bfloat16)
-
-    for s in range(n):
-        for a, r, length, block, p in segments(s, tokens):
-            s2[s, r:r + length, a * GROUP_DIM:(a + 1) * GROUP_DIM] = (
-                ybuf[p:p + length, block * GROUP_DIM:(block + 1) * GROUP_DIM]
-            )
-    returns = exchange(s2, r2, send2, recv2)
+        complete = []
+        for s in range(n):
+            runs = segments(s, tokens)
+            if s in returned or max(p + length for _, _, length, _, p in runs) > q + tile:
+                continue
+            returned.add(s)
+            complete.append(s)
+            for a, r, length, block, p in runs:
+                s2[s, r:r + length, a * GROUP_DIM:(a + 1) * GROUP_DIM] = (
+                    ybuf[p:p + length, block * GROUP_DIM:(block + 1) * GROUP_DIM]
+                )
+        for s in complete:
+            @pl.when(me != s)
+            def _():
+                give_back(s).start()
+
+            @pl.when(me == s)
+            def _():
+                pltpu.make_async_copy(s2.at[s], r2.at[s], recv2.at[s]).start()
 
     for j in range(pairs):
         for s in (2 * j, 2 * j + 1):
@@ -169,8 +185,12 @@
             bottom = jnp.where(lower, pltpu.roll(e, GROUP_DIM, 1), o)
             out[r:r + ROWS, cols] = (act[r:r + ROWS, cols] * top).astype(jnp.bfloat16)
             out[half + r:half + r + ROWS, cols] = (act[half + r:half + r + ROWS, cols] * bottom).astype(jnp.bfloat16)
-    for copy in sends + wcopies + returns:
+    for copy in sends + wcopies:
         copy.wait_send()
+    for s in range(n):
+        @pl.when(me != s)
+        def _():
+            give_back(s).wait_send()
 
 
 def solution(mesh):

time: 28.2 us -> 25.5 us (0.904)
  the two profiles are of different devices: /device:TPU:0 before, /device:TPU:28 now
where the time goes in v3:
time: 25.5 us; the launch traced here: 25.4 us
  Pallas kernels  24.6 us (96%)
  local copies, waits for them, and re-layouts  0.75 us (3%)
    pallas_call x1, Pallas kernels, local(): pl.pallas_call(functools.partial(kernel, n, dp, 256), out_shape=pltpu.VME...  24.6 us
    unnamed x1, local copies, waits for them, and re-layouts  0.75 us

profile of v3, /device:TPU:28, one launch (start us, length us, event | category | flops | bytes accessed | tf_op | source)
XLA Modules:
  0.0 25.4 jit_solution(8841402248314863839)
XLA Ops:
  0.0 24.6 %shard_map.64 = bf16[192,1024]{1,0:T(8,128)(2,1)S(1)} custom-call(bf16[192,1024]{1,0:T(8,128)(2,1)} %bitcast.8, bf16[192,1024]{1,0:T(8,128)(2,1)} %bitcast.9, f32[1,1024]{1,0:T(1,128)} %bitcast.10, f32[1,1024]{1,0:T(1,128)} %bitcast.11, bf16[512,1024]{1,0:T(8,128)(2,1)} %bitcast.7, f32[1,1024]{1,0:T(1,128)} %mbias.1), custom_call_target="tpu_custom_call" | custom-call | tf_op jit(solution)/shard_map/pallas_call | solution.py:210
  24.6 0.7 %copy.8 = bf16[1,192,1024]{2,1,0:T(8,128)(2,1)} copy(bf16[1,192,1024]{2,1,0:T(8,128)(2,1)S(1)} %bitcast.6) | data formatting | bytes 786432

commit v4 on v3

--- a/solution.py
+++ b/solution.py
@@ -43,7 +43,7 @@
 
 def kernel(
     n, dp, tile, value, gate, gain, nbias, weight, mbias, out,
-    vbuf, gbuf, gainbuf, nbiasbuf, mbiasbuf, act, full, bcol, s1, r1, xbuf, ybuf, s2, r2,
+    vbuf, gbuf, gainbuf, nbiasbuf, mbiasbuf, act, full, bcol, s1, r1, xbuf, s2, r2,
     load_sem, wsend, wrecv, send1, recv1, send2, recv2,
 ):
     me = lax.axis_index("sp")
@@ -68,7 +68,8 @@
     load_gate.start()
 
     barrier = pltpu.get_barrier_semaphore()
-    late = 2 * ((me * tokens + half) % SPAN) // SPAN
+    first = (me * tokens) % SPAN
+    late = ((3 * first) // (2 * SPAN)) * (1 - (first + tokens - 1) // SPAN)
     peers = [partner(me, k + late * (n - 2 * k), n) for k in range(n - 1, 0, -1)]
     for peer in peers:
         pl.semaphore_signal(barrier, inc=1, device_id={"sp": peer})
@@ -126,7 +127,7 @@
     load_mbias.wait()
     for q in range(0, SPAN, LANES):
         bcol[pl.ds(q, LANES), :] = jnp.transpose(jnp.broadcast_to(mbiasbuf[:, q:q + LANES], (LANES, LANES)))
-    xbuf[:, xbuf.shape[1] - LANES:] = jnp.zeros((SPAN, LANES), jnp.bfloat16)
+    xbuf[...] = jnp.zeros_like(xbuf)
 
     load_weight.wait()
     for j in range(1, dp):
@@ -137,42 +138,37 @@
         block = full[pl.ds(q, tile), pl.ds(q, tile)].astype(jnp.float32)
         keep = lax.broadcasted_iota(jnp.int32, (tile, tile), 1) <= lax.broadcasted_iota(jnp.int32, (tile, tile), 0)
         full[pl.ds(q, tile), pl.ds(q, tile)] = jnp.where(keep, block, 0.0).astype(jnp.bfloat16)
-
-    waited, returned = set(), set()
-    for q in range(0, SPAN, tile):
-        for s in range(n):
-            runs = segments(s, tokens)
-            if s in waited or min(p for _, _, _, _, p in runs) >= q + tile:
-                continue
-            waited.add(s)
-            pltpu.make_async_copy(s1.at[s], r1.at[s], recv1.at[s]).wait()
-            for a, r, length, block, p in runs:
-                xbuf[p:p + length, block * GROUP_DIM:(block + 1) * GROUP_DIM] = (
-                    r1[s, r:r + length, a * GROUP_DIM:(a + 1) * GROUP_DIM]
-                )
-        summed = jnp.dot(full[q:q + tile, :q + tile], xbuf[:q + tile, :], preferred_element_type=jnp.float32)
-        column = bcol[q:q + tile, :]
-        for j in range(0, xbuf.shape[1], LANES):
-            ybuf[q:q + tile, j:j + LANES] = (summed[:, j:j + LANES] + column).astype(jnp.bfloat16)
-        complete = []
-        for s in range(n):
-            runs = segments(s, tokens)
-            if s in returned or max(p + length for _, _, length, _, p in runs) > q + tile:
-                continue
-            returned.add(s)
-            complete.append(s)
-            for a, r, length, block, p in runs:
-                s2[s, r:r + length, a * GROUP_DIM:(a + 1) * GROUP_DIM] = (
-                    ybuf[p:p + length, block * GROUP_DIM:(block + 1) * GROUP_DIM]
-                )
-        for s in complete:
-            @pl.when(me != s)
-            def _():
-                give_back(s).start()
-
-            @pl.when(me == s)
-            def _():
-                pltpu.make_async_copy(s2.at[s], r2.at[s], recv2.at[s]).start()
+        if q + tile < SPAN:
+            full[q:q + tile, q + tile:] = jnp.zeros((tile, SPAN - q - tile), jnp.bfloat16)
+
+    waited = set()
+    last = {s: max(p + length for _, _, length, _, p in segments(s, tokens)) for s in range(n)}
+    for s in sorted(range(n), key=last.get):
+        for block in sorted({run[3] for run in segments(s, tokens)}):
+            mine = [run for run in segments(s, tokens) if run[3] == block]
+            begin = min(run[4] for run in mine)
+            end = max(run[4] + run[2] for run in mine)
+            for source in range(n):
+                runs = segments(source, tokens)
+                if source in waited or all(run[3] != block or run[4] >= end for run in runs):
+                    continue
+                waited.add(source)
+                pltpu.make_async_copy(s1.at[source], r1.at[source], recv1.at[source]).wait()
+                for a, r, length, into, p in runs:
+                    xbuf[into, p:p + length, :] = r1[source, r:r + length, a * GROUP_DIM:(a + 1) * GROUP_DIM]
+            depth = -(-end // LANES) * LANES
+            summed = jnp.dot(full[begin:end, :depth], xbuf[block, :depth, :], preferred_element_type=jnp.float32)
+            mixed = (summed + bcol[begin:end, :GROUP_DIM]).astype(jnp.bfloat16)
+            for a, r, length, _, p in mine:
+                s2[s, r:r + length, a * GROUP_DIM:(a + 1) * GROUP_DIM] = mixed[p - begin:p - begin + length, :]
+
+        @pl.when(me != s)
+        def _():
+            give_back(s).start()
+
+        @pl.when(me == s)
+        def _():
+            pltpu.make_async_copy(s2.at[s], r2.at[s], recv2.at[s]).start()
 
     for j in range(pairs):
         for s in (2 * j, 2 * j + 1):
@@ -202,7 +198,6 @@
         assert groups == 1 and span == SPAN and channels == n * GROUP_DIM and tokens % (2 * ROWS) == 0
         half = tokens // 2
         blocks = n * tokens // SPAN
-        width = -(-blocks * GROUP_DIM // LANES) * LANES
         packed = (n, half, 2 * GROUP_DIM)
         anywhere = pl.BlockSpec(memory_space=pl.ANY)
         bf16, f32 = jnp.bfloat16, jnp.float32
@@ -223,8 +218,7 @@
                 pltpu.VMEM((SPAN, LANES), f32),
                 pltpu.VMEM(packed, bf16),
                 pltpu.VMEM(packed, bf16),
-                pltpu.VMEM((SPAN, width), bf16),
-                pltpu.VMEM((SPAN, width), bf16),
+                pltpu.VMEM((blocks, SPAN, GROUP_DIM), bf16),
                 pltpu.VMEM(packed, bf16),
                 pltpu.VMEM(packed, bf16),
                 dma((6,)),

time: 25.5 us -> 25.7 us (level)
  the two profiles are of different devices: /device:TPU:28 before, /device:TPU:20 now
where the time goes in v4:
time: 25.7 us; the launch traced here: 25.5 us
  Pallas kernels  24.8 us (96%)
  local copies, waits for them, and re-layouts  0.75 us (3%)
    pallas_call x1, Pallas kernels, local(): pl.pallas_call(functools.partial(kernel, n, dp, 256), out_shape=pltpu.VME...  24.8 us
    unnamed x1, local copies, waits for them, and re-layouts  0.75 us

profile of v4, /device:TPU:20, one launch (start us, length us, event | category | flops | bytes accessed | tf_op | source)
XLA Modules:
  0.0 25.5 jit_solution(10605390945333294883)
XLA Ops:
  0.0 24.8 %shard_map.64 = bf16[192,1024]{1,0:T(8,128)(2,1)S(1)} custom-call(bf16[192,1024]{1,0:T(8,128)(2,1)} %bitcast.8, bf16[192,1024]{1,0:T(8,128)(2,1)} %bitcast.9, f32[1,1024]{1,0:T(1,128)} %bitcast.10, f32[1,1024]{1,0:T(1,128)} %bitcast.11, bf16[512,1024]{1,0:T(8,128)(2,1)} %bitcast.7, f32[1,1024]{1,0:T(1,128)} %mbias.1), custom_call_target="tpu_custom_call" | custom-call | tf_op jit(solution)/shard_map/pallas_call | solution.py:205
  24.8 0.7 %copy.8 = bf16[1,192,1024]{2,1,0:T(8,128)(2,1)} copy(bf16[1,192,1024]{2,1,0:T(8,128)(2,1)S(1)} %bitcast.6) | data formatting | bytes 786432
